TPU v7x, 32 devices: a whole 2x2x4 slice. The times are simulated.
32 devices in a mesh: sp: 8 (over z, y), tp: 4 (over x, core).
Axes of the slice: x: 2, y: 2, z: 4, core: 2. Of those that a mesh axis runs over, the one named last changes fastest.
Arguments:
- gate_in: bfloat16 [4096, 2048], P('sp', 'tp'), may hold values from -6 to 6
- value_in: bfloat16 [4096, 2048], P('sp', 'tp'), may hold values from -6 to 6
- gate_out: bfloat16 [4096, 2048], P('sp', 'tp'), may hold values from -6 to 6
- conv_taps: float32 [3, 2048], P(None, 'tp'), may hold values from -3.5 to 3.5
- proj_weight: bfloat16 [2048, 2048], P('tp'), may hold values from -0.125 to 0.125
- residual: bfloat16 [4096, 2048], P(('sp', 'tp')), may hold values from -6 to 6
- norm_gain: float32 [2048], replicated, may hold values from 0.1 to 1.9
- routes: int32 [4096, 2], P('sp'), may hold values from 0 to 7, all different within a row; in each aligned block of 128 rows (0 to 127, 128 to 255, ...) at most 64 rows name the same one
- route_weight: float32 [4096, 2], P('sp'), may hold values from 0.1 to 0.9
- expert_gate: bfloat16 [8, 2048, 2048], P('sp', None, 'tp'), may hold values from -0.125 to 0.125
- expert_up: bfloat16 [8, 2048, 2048], P('sp', None, 'tp'), may hold values from -0.125 to 0.125
- expert_down: bfloat16 [8, 2048, 2048], P('sp', 'tp'), may hold values from -0.125 to 0.125
Outputs:
- layer_out: bfloat16 [4096, 2048], P(('sp', 'tp'))
Inputs may be any that keep to these rules, and one draw needn't show every extreme that they name: `routes`: A token's 2 experts differ. In each aligned block of 128 tokens no expert is named by more than 64 tokens, a bound that some block reaches.
All inputs are finite; a program needn't handle non-finite values.
Results may differ from a plain program's by a relative error of at most 0.012.
Values may be sent and summed in bfloat16 or wider, within the bound.
A program may use at most 128 MiB of HBM per device.

v0:
```python
import jax
import jax.numpy as jnp
from jax import lax
from jax.sharding import PartitionSpec as P


def passed_along(shard, axis, by):
    size = lax.axis_size(axis)
    pairs = [(i, i + by) for i in range(size) if 0 <= i + by < size]
    return lax.ppermute(shard, axis, pairs)


def rounded(values):
    return lax.optimization_barrier(values.astype(jnp.bfloat16)).astype(jnp.float32)


def slot_numbers(route_ids, block_rows, expert_count):
    block_count = route_ids.shape[0] // block_rows
    flat_ids = route_ids.reshape(block_count, block_rows * route_ids.shape[1])
    one_hot = (
        flat_ids[:, :, None] == jnp.arange(expert_count, dtype=jnp.int32)[None, None, :]
    ).astype(jnp.int32)
    before = jnp.cumsum(one_hot, axis=1) - one_hot
    return jnp.sum(before * one_hot, axis=2).reshape(route_ids.shape)


def normalize(hidden_rows, norm_gain):
    inverse = lax.rsqrt(jnp.mean(hidden_rows * hidden_rows, axis=-1, keepdims=True) + 1e-05)
    return (hidden_rows * inverse * norm_gain).astype(jnp.bfloat16)


def dispatch_rows(normed, route_ids, block_rows, expert_count, capacity):
    row_count = route_ids.shape[0]
    top_count = route_ids.shape[1]
    block_count = row_count // block_rows
    slots = slot_numbers(route_ids, block_rows, expert_count)
    row_ids = jnp.arange(row_count, dtype=jnp.int32)
    flat_index = ((row_ids // block_rows)[:, None] * expert_count + route_ids) * capacity + slots
    slot_token = (
        jnp.full((block_count * expert_count * capacity,), row_count, jnp.int32)
        .at[flat_index.reshape(-1)]
        .set(jnp.repeat(row_ids, top_count))
    )
    padded_rows = jnp.concatenate([normed, jnp.zeros((1, normed.shape[1]), jnp.bfloat16)], axis=0)
    outgoing = padded_rows[slot_token].reshape(block_count, expert_count, capacity, normed.shape[1])
    return (outgoing, slots)


def body(
    gate_in,
    value_in,
    gate_out,
    conv_taps,
    proj_weight,
    residual,
    norm_gain,
    routes,
    route_weight,
    expert_gate,
    expert_up,
    expert_down,
):
    tok_dev = gate_in.shape[0]
    model_width = residual.shape[1]
    tp_count = lax.axis_size("tp")
    groups = lax.axis_size("sp")
    quarter = residual.shape[0]
    top_count = routes.shape[1]
    capacity = 2 * quarter * top_count // groups
    tp_index = lax.axis_index("tp")
    first_own = tp_index * quarter
    prior_gate, prior_value = passed_along(
        (gate_in[tok_dev - 2 :], value_in[tok_dev - 2 :]), "sp", 1
    )
    product = gate_in.astype(jnp.float32) * value_in.astype(jnp.float32)
    prior_mix = prior_gate.astype(jnp.float32) * prior_value.astype(jnp.float32)
    padded = jnp.concatenate([prior_mix, product], axis=0)
    conv_sum = conv_taps[0] * padded[:-2] + conv_taps[1] * padded[1:-1] + conv_taps[2] * padded[2:]
    mixed_out = (gate_out.astype(jnp.float32) * conv_sum).astype(jnp.bfloat16)
    own_routes = lax.dynamic_slice_in_dim(routes, first_own, quarter, 0)
    own_weights = lax.dynamic_slice_in_dim(route_weight, first_own, quarter, 0)
    row_block = mixed_out
    summed = lax.psum_scatter(
        rounded(jnp.dot(row_block, proj_weight, preferred_element_type=jnp.float32)).astype(
            jnp.bfloat16
        ),
        "tp",
        scatter_dimension=0,
        tiled=True,
    ).astype(jnp.float32)
    my_rows = residual.astype(jnp.float32) + summed
    normed = normalize(my_rows, norm_gain)
    outgoing, own_slots = dispatch_rows(normed, own_routes, quarter, groups, capacity)
    own_arrived = lax.all_to_all(outgoing, "sp", split_axis=1, concat_axis=1, tiled=True)
    received = lax.all_gather(own_arrived, "tp", axis=0, tiled=True)
    flat_rows = received.reshape(tp_count * groups * capacity, model_width)
    gate_weight = expert_gate[0]
    up_weight = expert_up[0]
    down_weight = expert_down[0]
    row_block = flat_rows
    gate_pre = jnp.dot(row_block, gate_weight, preferred_element_type=jnp.float32)
    up_pre = jnp.dot(row_block, up_weight, preferred_element_type=jnp.float32)
    hidden = (jax.nn.silu(gate_pre) * up_pre).astype(jnp.bfloat16)
    expert_rows = lax.psum_scatter(
        rounded(jnp.dot(hidden, down_weight, preferred_element_type=jnp.float32)).astype(
            jnp.bfloat16
        ),
        "tp",
        scatter_dimension=0,
        tiled=True,
    )
    returned = lax.all_to_all(
        expert_rows.reshape(groups, capacity, model_width),
        "sp",
        split_axis=0,
        concat_axis=0,
        tiled=True,
    )
    flat_pick = own_routes * capacity + own_slots
    picked = returned.reshape(groups * capacity, model_width)[flat_pick]
    weighted = jnp.sum(own_weights[:, :, None] * picked.astype(jnp.float32), axis=1)
    return (my_rows + weighted).astype(jnp.bfloat16)


def solution(mesh):
    placed = (
        P("sp", "tp"),
        P("sp", "tp"),
        P("sp", "tp"),
        P(None, "tp"),
        P("tp", None),
        P(("sp", "tp"), None),
        P(),
        P("sp", None),
        P("sp", None),
        P("sp", None, "tp"),
        P("sp", None, "tp"),
        P("sp", "tp", None),
    )
    return jax.shard_map(
        body, mesh=mesh, in_specs=placed, out_specs=P(("sp", "tp"), None), check_vma=False
    )
```

profile of v0, /device:TPU:0, one launch (start us, length us, event | category | flops | bytes accessed | tf_op | source)
XLA Modules:
  0.0 337.2 jit_solution(5291792366952498572)
XLA Ops:
  6.5 0.0 copy-start
  6.5 0.0 reduce-scatter.3.cloned.1.call-start
  6.5 0.9 slice.28
  7.4 5.0 %collective-permute-start = (bf16[2,512]{1,0:T(2,128)(2,1)S(1)}, bf16[2,512]{1,0:T(2,128)(2,1)S(1)}, u32[]{:S(2)}, u32[]{:S(2)}) collective-permute-start(bf16[2,512]{1,0:T(2,128)(2,1)S(1)} %slice.28), channel_id=1, source_target_pairs={{0,4},{4,8},{8,12},{12,16},{16,20},{20,24},{24,28},{1,5},{5,9},{9,... | collective-permute-start | bytes 6152 | tf_op jit(solution)/shard_map/ppermute | solution.py:10
  12.4 0.7 slice.29
  13.1 3.4 %collective-permute-start.1 = (bf16[2,512]{1,0:T(2,128)(2,1)S(1)}, bf16[2,512]{1,0:T(2,128)(2,1)S(1)}, u32[]{:S(2)}, u32[]{:S(2)}) collective-permute-start(bf16[2,512]{1,0:T(2,128)(2,1)S(1)} %slice.29), channel_id=1, source_target_pairs={{0,4},{4,8},{8,12},{12,16},{16,20},{20,24},{24,28},{1,5},{5,9},{9,... | collective-permute-start | bytes 6152 | tf_op jit(solution)/shard_map/ppermute | solution.py:10
  16.6 1.3 convert_multiply_fusion
  17.9 0.0 copy-done.4
  17.9 0.0 collective-permute-done
  17.9 0.0 collective-permute-done.1
  18.0 0.0 copy-done.6
  18.0 3.8 %convolution_convert_fusion.1 = bf16[512,2048]{1,0:T(8,128)(2,1)} fusion(bf16[512,2048]{1,0:T(8,128)(2,1)S(1)} %copy-done.6, f32[2,512]{1,0:T(2,128)S(1)} %convert_multiply_fusion.1, f32[512,512]{1,0:T(8,128)S(1)} %convert_multiply_fusion, bf16[512,512]{1,0:T(8,128)(2,1)} %param.14, f32[512]{0:T(512)S(1)} %bitcast.44, f32[512]{0:T(512)S(1)} %bitcast.45, ...), kind=kOutput, calls=%fused_computation.5 | convolution fusion | flops 1077411840 | bytes 5777408 | tf_op jit(solution)/shard_map/dot_general | solution.py:84
  21.8 0.0 reduce-scatter.3.cloned.1.call-update
  21.8 0.0 all-gather.2.cloned.1.call-start
  21.9 0.7 constant_dynamic-slice_fusion
  22.6 0.1 copy.20
  22.7 0.1 eq.27
  22.9 0.6 reduce-window.6
  23.5 0.2 slice_reduce_fusion
  23.7 0.1 fusion.16
  23.8 0.1 reshape.195
  24.0 0.1 compare_select_fusion
  24.1 0.1 reshape.196
  24.2 0.1 reshape.222
  24.4 1.4 scatter_custom_fusion
  25.8 29.2 %reduce-scatter.3.cloned.1.call-done = bf16[128,2048]{1,0:T(8,128)(2,1)} async-done(((bf16[512,2048]{1,0:T(8,128)(2,1)}), bf16[128,2048]{1,0:T(8,128)(2,1)}) %reduce-scatter.3.cloned.1.call-update) | async-done | bytes 524304 | tf_op jit(solution)/shard_map/reduce_scatter | solution.py:83
  55.0 1.3 multiply_reduce_fusion.1
  56.3 0.0 copy-done.3
  56.3 1.3 multiply_convert_fusion.1
  57.6 3.3 gather_fusion
  61.0 53.7 %all_to_all.10 = bf16[1,8,64,2048]{3,2,0,1:T(8,128)(2,1)} all-to-all(bf16[1,8,64,2048]{3,2,0,1:T(8,128)(2,1)} %bitcast.39), channel_id=1, replica_groups=mesh['sp'=8,'tp'=4] {'sp'}, dimensions={1} | all-to-all | bytes 4194304 | tf_op jit(solution)/shard_map/all_to_all | solution.py:94
  114.7 0.0 all-gather.2.cloned.1.call-update
  114.7 0.0 reduce-scatter.5.cloned.1.call-start
  114.8 56.4 %all-gather.2.cloned.1.call-done = bf16[4,8,64,2048]{3,2,1,0:T(8,128)(2,1)} async-done(((bf16[1,8,64,2048]{3,2,1,0:T(8,128)(2,1)}), bf16[4,8,64,2048]{3,2,1,0:T(8,128)(2,1)}) %all-gather.2.cloned.1.call-update) | async-done | bytes 8388624 | tf_op jit(solution)/shard_map/all_gather | solution.py:95
  171.2 7.7 %fusion.2 = f32[2048,512]{1,0:T(8,128)S(1)} fusion(bf16[2048,2048]{1,0:T(8,128)(2,1)} %bitcast.47, bf16[1,2048,512]{2,1,0:T(8,128)(2,1)} %param.21), kind=kOutput, calls=%fused_computation.8 | convolution fusion | flops 4294967296 | bytes 14680064 | tf_op jit(solution)/shard_map/dot_general | solution.py:101
  178.9 5.2 %multiply_convert_fusion = bf16[2048,512]{1,0:T(8,128)(2,1)S(1)} fusion(f32[2048,512]{1,0:T(8,128)S(1)} %fusion.2, bf16[2048,2048]{1,0:T(8,128)(2,1)S(1)} %bitcast.48, bf16[1,2048,512]{2,1,0:T(8,128)(2,1)S(1)} %copy-done.7), kind=kOutput, calls=%fused_computation.4 | convolution fusion | flops 4301258752 | bytes 16777216 | tf_op jit(solution)/shard_map/dot_general | solution.py:102
  184.1 6.8 %convolution_convert_fusion = bf16[2048,2048]{1,0:T(8,128)(2,1)} fusion(bf16[2048,512]{1,0:T(8,128)(2,1)S(1)} %multiply_convert_fusion, bf16[1,512,2048]{2,1,0:T(8,128)(2,1)S(1)} %copy-done), kind=kOutput, calls=%fused_computation.3 | convolution fusion | flops 4299161600 | bytes 12582912 | tf_op jit(solution)/shard_map/dot_general | solution.py:105
  190.9 0.0 reduce-scatter.5.cloned.1.call-update
  190.9 71.5 %reduce-scatter.5.cloned.1.call-done = bf16[512,2048]{1,0:T(8,128)(2,1)} async-done(((bf16[2048,2048]{1,0:T(8,128)(2,1)}), bf16[512,2048]{1,0:T(8,128)(2,1)}) %reduce-scatter.5.cloned.1.call-update) | async-done | bytes 2097168 | tf_op jit(solution)/shard_map/reduce_scatter | solution.py:104
  262.5 5.5 %all-to-all-start.1 = ((bf16[8,64,2048]{2,1,0:T(8,128)(2,1)}), bf16[8,64,2048]{2,1,0:T(8,128)(2,1)}, u32[]{:S(2)}, u32[]{:S(2)}) async-start(bf16[8,64,2048]{2,1,0:T(8,128)(2,1)} %bitcast.41), calls=%async_computation.3 | async-start | bytes 4194304 | tf_op jit(solution)/shard_map/all_to_all | solution.py:112
  268.0 0.1 reshape.212
  268.1 0.7 constant_dynamic-slice_fusion.1
  268.8 0.1 copy.16
  268.9 47.2 %all-to-all-done.1 = bf16[8,64,2048]{2,1,0:T(8,128)(2,1)} async-done(((bf16[8,64,2048]{2,1,0:T(8,128)(2,1)}), bf16[8,64,2048]{2,1,0:T(8,128)(2,1)}, u32[]{:S(2)}, u32[]{:S(2)}) %all-to-all-start.1) | async-done | bytes 2097184 | tf_op jit(solution)/shard_map/all_to_all | solution.py:112
  316.2 5.2 %gather_fusion.1 = bf16[256,2048]{1,0:T(8,128)(2,1)} fusion(bf16[512,2048]{1,0:T(8,128)(2,1)} %bitcast.18, s32[1024]{0:T(1024)S(1)} %pad_clamp_fusion), kind=kCustom, calls=%fused_computation.1 | custom fusion | bytes 2098176 | tf_op jit(solution)/shard_map/gather | solution.py:120
  321.4 3.4 %reshape.229 = f32[128,2,2048]{2,1,0:T(2,128)} reshape(bf16[256,2048]{1,0:T(8,128)(2,1)} %gather_fusion.1) | data formatting | bytes 3145728 | tf_op jit(solution)/shard_map/convert_element_type | solution.py:121
  324.8 4.9 %multiply_reduce_fusion = f32[128,2048]{1,0:T(8,128)S(1)} fusion(f32[128,2,2048]{2,1,0:T(2,128)} %reshape.229, f32[128,2]{1,0:T(8,128)S(1)} %copy.16), kind=kLoop, calls=%fused_computation.10 | loop fusion | flops 786432 | bytes 3146752 | tf_op jit(solution)/shard_map/reduce_sum | solution.py:121
  329.7 1.0 add_convert_fusion
  (25 shorter events, 0.2 us)
Async XLA Ops:
  6.5 177.6 %copy-start = (bf16[1,512,2048]{2,1,0:T(8,128)(2,1)S(1)}, bf16[1,512,2048]{2,1,0:T(8,128)(2,1)}, u32[]{:S(2)}) copy-start(bf16[1,512,2048]{2,1,0:T(8,128)(2,1)} %param.23) | copy-start | bytes 6291460
  6.5 11.4 %copy-start.4 = (f32[3,512]{1,0:T(4,128)S(1)}, f32[3,512]{1,0:T(4,128)}, u32[]{:S(2)}) copy-start(f32[3,512]{1,0:T(4,128)} %param.15) | copy-start | bytes 18436
  6.5 48.5 %reduce-scatter.3.cloned.1.call-start = ((), (), s32[]{:S(2)}) async-start(), calls=%async_computation.4 | async-start | bytes 2621440 | tf_op jit(solution)/shard_map/reduce_scatter | solution.py:83
  6.5 11.4 %copy-start.6 = (bf16[512,2048]{1,0:T(8,128)(2,1)S(1)}, bf16[512,2048]{1,0:T(8,128)(2,1)}, u32[]{:S(2)}) copy-start(bf16[512,2048]{1,0:T(8,128)(2,1)} %param.16) | copy-start | bytes 6291460
  7.4 10.5 %collective-permute-start = (bf16[2,512]{1,0:T(2,128)(2,1)S(1)}, bf16[2,512]{1,0:T(2,128)(2,1)S(1)}, u32[]{:S(2)}, u32[]{:S(2)}) collective-permute-start(bf16[2,512]{1,0:T(2,128)(2,1)S(1)} %slice.28), channel_id=1, source_target_pairs={{0,4},{4,8},{8,12},{12,16},{16,20},{20,24},{24,28},{1,5},{5,9},{9,... | collective-permute-start | bytes 6152 | tf_op jit(solution)/shard_map/ppermute | solution.py:10
  13.1 4.8 %collective-permute-start.1 = (bf16[2,512]{1,0:T(2,128)(2,1)S(1)}, bf16[2,512]{1,0:T(2,128)(2,1)S(1)}, u32[]{:S(2)}, u32[]{:S(2)}) collective-permute-start(bf16[2,512]{1,0:T(2,128)(2,1)S(1)} %slice.29), channel_id=1, source_target_pairs={{0,4},{4,8},{8,12},{12,16},{16,20},{20,24},{24,28},{1,5},{5,9},{9,... | collective-permute-start | bytes 6152 | tf_op jit(solution)/shard_map/ppermute | solution.py:10
  21.8 33.2 %copy-start.1 = (bf16[128,2048]{1,0:T(8,128)(2,1)S(1)}, bf16[128,2048]{1,0:T(8,128)(2,1)}, u32[]{:S(2)}) copy-start(bf16[128,2048]{1,0:T(8,128)(2,1)} %param.17) | copy-start | bytes 1572868
  21.8 34.5 %copy-start.3 = (f32[2048]{0:T(1024)S(1)}, f32[2048]{0:T(1024)}, u32[]{:S(2)}) copy-start(f32[2048]{0:T(1024)} %param.18) | copy-start | bytes 24580
  21.8 149.4 %all-gather.2.cloned.1.call-start = ((), (), s32[]{:S(2)}) async-start(), calls=%async_computation.5 | async-start | bytes 10485760 | tf_op jit(solution)/shard_map/all_gather | solution.py:95
  114.7 147.8 %reduce-scatter.5.cloned.1.call-start = ((), (), s32[]{:S(2)}) async-start(), calls=%async_computation.6 | async-start | bytes 10485760 | tf_op jit(solution)/shard_map/reduce_scatter | solution.py:104
  171.2 7.7 %copy-start.5 = (bf16[4,8,64,2048]{3,2,1,0:T(8,128)(2,1)S(1)}, bf16[4,8,64,2048]{3,2,1,0:T(8,128)(2,1)}, u32[]{:S(2)}) copy-start(bf16[4,8,64,2048]{3,2,1,0:T(8,128)(2,1)} %all-gather.2.cloned.1.call-done) | copy-start | bytes 25165828
  171.2 7.7 %copy-start.7 = (bf16[1,2048,512]{2,1,0:T(8,128)(2,1)S(1)}, bf16[1,2048,512]{2,1,0:T(8,128)(2,1)}, u32[]{:S(2)}) copy-start(bf16[1,2048,512]{2,1,0:T(8,128)(2,1)} %param.22) | copy-start | bytes 6291460
  262.5 53.7 %all-to-all-start.1 = ((bf16[8,64,2048]{2,1,0:T(8,128)(2,1)}), bf16[8,64,2048]{2,1,0:T(8,128)(2,1)}, u32[]{:S(2)}, u32[]{:S(2)}) async-start(bf16[8,64,2048]{2,1,0:T(8,128)(2,1)} %bitcast.41), calls=%async_computation.3 | async-start | bytes 4194304 | tf_op jit(solution)/shard_map/all_to_all | solution.py:112
  324.8 4.9 %copy-start.2 = (bf16[128,2048]{1,0:T(8,128)(2,1)S(1)}, bf16[128,2048]{1,0:T(8,128)(2,1)}, u32[]{:S(2)}) copy-start(bf16[128,2048]{1,0:T(8,128)(2,1)} %reduce-scatter.3.cloned.1.call-done) | copy-start | bytes 1572868
Sparse Core Ops, SparseCore 0:
  22.0 32.9 reduce-scatter.2
  114.8 56.3 all-gather.1
  191.0 71.3 reduce-scatter.4
where the time goes:
time: 338 us; the launch traced here: 337 us
  waiting for transfers between devices  204 us (60%)
  blocking collectives  53.7 us (16%)
  matrix products  23.5 us (7%)
  local copies, waits for them, and re-layouts  17.5 us (5%)
  starting transfers between devices  14 us (4%)
  between operations  13.3 us (4%)
  other arithmetic  10.6 us (3%)
    reduce_scatter x1, waiting for transfers between devices, body(): lax.psum_scatter(rounded(jnp.dot(hidden, down_weight, preferred_element_t...  71.5 us
    all_gather x1, waiting for transfers between devices, body(): received = lax.all_gather(own_arrived, 'tp', axis=0, tiled=True)  56.4 us
    all_to_all x1, blocking collectives, body(): lax.all_to_all(outgoing, 'sp', split_axis=1, concat_axis=1, tiled=True)  53.7 us
    all_to_all x1, waiting for transfers between devices, body(): lax.all_to_all(expert_rows.reshape(groups, capacity, model_width), 'sp',...  47.2 us
    reduce_scatter x1, waiting for transfers between devices, body(): lax.psum_scatter(rounded(jnp.dot(row_block, proj_weight, preferred_elemen...  29.2 us
    ppermute x2, starting transfers between devices, passed_along(): return lax.ppermute(shard, axis, pairs)  8.43 us
    dot_general x1, matrix products, body(): jnp.dot(row_block, gate_weight, preferred_element_type=jnp.float32)  7.67 us
    dot_general x1, matrix products, body(): jnp.dot(hidden, down_weight, preferred_element_type=jnp.float32)  6.79 us
  transfers between devices with their start and end apart: 6, of which 4 were waited for; matrix products, arithmetic and copies ran while one was open for 2% of the time, Pallas kernels for 0%

commit v1 on v0

--- a/solution.py
+++ b/solution.py
@@ -92,7 +92,12 @@
     normed = normalize(my_rows, norm_gain)
     outgoing, own_slots = dispatch_rows(normed, own_routes, quarter, groups, capacity)
     own_arrived = lax.all_to_all(outgoing, "sp", split_axis=1, concat_axis=1, tiled=True)
-    received = lax.all_gather(own_arrived, "tp", axis=0, tiled=True)
+    ring = [own_arrived]
+    for hop in range(3):
+        ring.append(lax.ppermute(ring[-1], "tp", [(dev, (dev + 1) % 4) for dev in range(4)]))
+    received = jnp.roll(
+        jnp.concatenate(ring[::-1], axis=0), (lax.axis_index("tp") + 1) * ring[0].shape[0], axis=0
+    )
     flat_rows = received.reshape(tp_count * groups * capacity, model_width)
     gate_weight = expert_gate[0]
     up_weight = expert_up[0]

time: 338 us -> 387 us (1.14)
  local copies, waits for them, and re-layouts: 17.5 us -> 48.2 us
  waiting for transfers between devices: 204 us -> 222 us
    ppermute x0 -> x3, waiting for transfers between devices: none -> 76.8 us  [body(): lax.ppermute(ring[-1], 'tp', [(dev, (dev + 1) % 4) for dev in range(4)])]
    all_gather x1 -> x0, waiting for transfers between devices: 56.4 us -> none  [body(): received = lax.all_gather(own_arrived, 'tp', axis=0, tiled=True)]
    unnamed x17 -> x30, local copies, waits for them, and re-layouts: 0.15 us -> 20.1 us
    dynamic_slice x0 -> x1, local copies, waits for them, and re-layouts: none -> 8.41 us  [body(): jnp.roll(jnp.concatenate(ring[::-1], axis=0), (lax.axis_index('tp') + 1)...]
  transfers between devices with their start and end apart: 6 -> 8, of which waited for: 4 -> 6; matrix products, arithmetic and copies ran while one was open for 2% -> 2% of each run, Pallas kernels for 0% -> 0%
where the time goes in v1:
time: 387 us; the launch traced here: 386 us
  waiting for transfers between devices  222 us (57%)
  blocking collectives  53.6 us (14%)
  local copies, waits for them, and re-layouts  48.2 us (12%)
  matrix products  24.1 us (6%)
  starting transfers between devices  13.9 us (4%)
  between operations  13.6 us (4%)
  other arithmetic  10.6 us (3%)
    ppermute x3, waiting for transfers between devices, body(): lax.ppermute(ring[-1], 'tp', [(dev, (dev + 1) % 4) for dev in range(4)])  76.8 us
    reduce_scatter x1, waiting for transfers between devices, body(): lax.psum_scatter(rounded(jnp.dot(hidden, down_weight, preferred_element_t...  69.6 us
    all_to_all x1, blocking collectives, body(): lax.all_to_all(outgoing, 'sp', split_axis=1, concat_axis=1, tiled=True)  53.6 us
    all_to_all x1, waiting for transfers between devices, body(): lax.all_to_all(expert_rows.reshape(groups, capacity, model_width), 'sp',...  47.2 us
    reduce_scatter x1, waiting for transfers between devices, body(): lax.psum_scatter(rounded(jnp.dot(row_block, proj_weight, preferred_elemen...  28.4 us
    unnamed x30, local copies, waits for them, and re-layouts  20.1 us
    dynamic_slice x1, local copies, waits for them, and re-layouts, body(): jnp.roll(jnp.concatenate(ring[::-1], axis=0), (lax.axis_index('tp') + 1)...  8.41 us
    ppermute x2, starting transfers between devices, passed_along(): return lax.ppermute(shard, axis, pairs)  8.3 us
  transfers between devices with their start and end apart: 8, of which 6 were waited for; matrix products, arithmetic and copies ran while one was open for 2% of the time, Pallas kernels for 0%

profile of v1, /device:TPU:0, one launch (start us, length us, event | category | flops | bytes accessed | tf_op | source)
XLA Modules:
  0.0 386.1 jit_solution(16566651305927072678)
XLA Ops:
  6.5 0.9 slice.28
  7.4 4.9 %collective-permute-start = (bf16[2,512]{1,0:T(2,128)(2,1)S(1)}, bf16[2,512]{1,0:T(2,128)(2,1)S(1)}, u32[]{:S(2)}, u32[]{:S(2)}) collective-permute-start(bf16[2,512]{1,0:T(2,128)(2,1)S(1)} %slice.28), channel_id=1, source_target_pairs={{0,4},{4,8},{8,12},{12,16},{16,20},{20,24},{24,28},{1,5},{5,9},{9,... | collective-permute-start | bytes 6152 | tf_op jit(solution)/shard_map/ppermute | solution.py:10
  12.3 0.7 slice.29
  13.0 3.4 collective-permute-start.1
  16.4 1.3 convert_multiply_fusion
  17.8 0.8 fusion.21
  18.6 4.6 %convolution_convert_fusion.1 = bf16[512,2048]{1,0:T(8,128)(2,1)} fusion(bf16[512,2048]{1,0:T(8,128)(2,1)} %param.16, f32[2,512]{1,0:T(2,128)S(1)} %convert_multiply_fusion.1, f32[512,512]{1,0:T(8,128)S(1)} %convert_multiply_fusion, bf16[512,512]{1,0:T(8,128)(2,1)} %param.14, f32[512]{0:T(512)S(1)} %bitcast.50, f32[512]{0:T(512)S(1)} %bitcast.51, ...), kind=kOutput, calls=%fused_computation.5 | convolution fusion | flops 1077411840 | bytes 5777408 | tf_op jit(solution)/shard_map/dot_general | solution.py:84
  23.3 0.7 constant_dynamic-slice_fusion.1
  24.0 0.1 copy.25
  24.1 0.1 eq.30
  24.2 0.6 reduce-window.6
  24.8 0.2 slice_reduce_fusion
  25.2 0.1 reshape.195
  25.4 0.1 reshape.196
  25.6 0.1 reshape.222
  25.7 1.4 scatter_custom_fusion
  27.2 28.4 %reduce-scatter.3.cloned.1.call-done = bf16[128,2048]{1,0:T(8,128)(2,1)} async-done(((bf16[512,2048]{1,0:T(8,128)(2,1)}), bf16[128,2048]{1,0:T(8,128)(2,1)}) %reduce-scatter.3.cloned.1.call-update) | async-done | bytes 524304 | tf_op jit(solution)/shard_map/reduce_scatter | solution.py:83
  55.6 1.3 multiply_reduce_fusion.1
  56.9 1.3 multiply_convert_fusion.1
  58.2 3.3 gather_fusion
  61.6 53.6 %all_to_all.10 = bf16[1,8,64,2048]{3,2,0,1:T(8,128)(2,1)S(1)} all-to-all(bf16[1,8,64,2048]{3,2,0,1:T(8,128)(2,1)} %bitcast.46), channel_id=1, replica_groups=mesh['sp'=8,'tp'=4] {'sp'}, dimensions={1} | all-to-all | bytes 4194304 | tf_op jit(solution)/shard_map/all_to_all | solution.py:94
  115.2 1.3 copy-done.1
  116.5 25.5 %collective-permute-done.2 = bf16[1,8,64,2048]{3,2,1,0:T(8,128)(2,1)S(1)} collective-permute-done((bf16[1,8,64,2048]{3,2,1,0:T(8,128)(2,1)S(1)}, bf16[1,8,64,2048]{3,2,1,0:T(8,128)(2,1)S(1)}, u32[]{:S(2)}, u32[]{:S(2)}) %collective-permute-start.2) | collective-permute-done | bytes 2097184 | tf_op jit(solution)/shard_map/ppermute | solution.py:97
  141.9 1.3 copy-done.4
  143.3 25.6 %collective-permute-done.3 = bf16[1,8,64,2048]{3,2,1,0:T(8,128)(2,1)} collective-permute-done((bf16[1,8,64,2048]{3,2,1,0:T(8,128)(2,1)S(1)}, bf16[1,8,64,2048]{3,2,1,0:T(8,128)(2,1)}, u32[]{:S(2)}, u32[]{:S(2)}) %collective-permute-start.3) | collective-permute-done | bytes 2097184 | tf_op jit(solution)/shard_map/ppermute | solution.py:97
  168.8 25.8 %collective-permute-done.4 = bf16[1,8,64,2048]{3,2,1,0:T(8,128)(2,1)} collective-permute-done((bf16[1,8,64,2048]{3,2,1,0:T(8,128)(2,1)}, bf16[1,8,64,2048]{3,2,1,0:T(8,128)(2,1)}, u32[]{:S(2)}, u32[]{:S(2)}) %collective-permute-start.4) | collective-permute-done | bytes 2097184 | tf_op jit(solution)/shard_map/ppermute | solution.py:97
  194.6 3.2 constant_dynamic-update-slice_fusion.7
  197.8 3.3 constant_dynamic-update-slice_fusion.6
  201.1 1.5 constant_dynamic-update-slice_fusion.5
  202.6 1.5 constant_dynamic-update-slice_fusion.4
  204.0 3.2 constant_dynamic-update-slice_fusion.3
  207.3 3.1 constant_dynamic-update-slice_fusion.2
  210.4 1.5 constant_dynamic-update-slice_fusion.1
  211.9 1.5 constant_dynamic-update-slice_fusion
  213.4 8.4 %constant_dynamic-slice_fusion = bf16[4,8,64,2048]{3,2,1,0:T(8,128)(2,1)} fusion(bf16[8,8,64,2048]{3,2,1,0:T(8,128)(2,1)} %constant_dynamic-update-slice_fusion, s32[]{:T(128)S(6)} %select_n.47), kind=kLoop, calls=%fused_computation.58 | loop fusion | bytes 16777220 | tf_op jit(solution)/shard_map/jit(_roll_dynamic)/dynamic_slice | solution.py:98
  221.8 7.7 %fusion.2 = f32[2048,512]{1,0:T(8,128)S(1)} fusion(bf16[2048,2048]{1,0:T(8,128)(2,1)} %bitcast.44, bf16[1,2048,512]{2,1,0:T(8,128)(2,1)S(1)} %copy-done.9), kind=kOutput, calls=%fused_computation.8 | convolution fusion | flops 4294967296 | bytes 14680064 | tf_op jit(solution)/shard_map/dot_general | solution.py:106
  229.5 5.2 %multiply_convert_fusion = bf16[2048,512]{1,0:T(8,128)(2,1)S(1)} fusion(f32[2048,512]{1,0:T(8,128)S(1)} %fusion.2, bf16[2048,2048]{1,0:T(8,128)(2,1)S(1)} %bitcast.45, bf16[1,2048,512]{2,1,0:T(8,128)(2,1)S(1)} %copy-done.10), kind=kOutput, calls=%fused_computation.4 | convolution fusion | flops 4301258752 | bytes 16777216 | tf_op jit(solution)/shard_map/dot_general | solution.py:107
  234.7 6.7 %convolution_convert_fusion = bf16[2048,2048]{1,0:T(8,128)(2,1)} fusion(bf16[2048,512]{1,0:T(8,128)(2,1)S(1)} %multiply_convert_fusion, bf16[1,512,2048]{2,1,0:T(8,128)(2,1)S(1)} %copy-done), kind=kOutput, calls=%fused_computation.3 | convolution fusion | flops 4299161600 | bytes 12582912 | tf_op jit(solution)/shard_map/dot_general | solution.py:110
  241.4 69.6 %reduce-scatter.5.cloned.1.call-done = bf16[512,2048]{1,0:T(8,128)(2,1)} async-done(((bf16[2048,2048]{1,0:T(8,128)(2,1)}), bf16[512,2048]{1,0:T(8,128)(2,1)}) %reduce-scatter.5.cloned.1.call-update) | async-done | bytes 2097168 | tf_op jit(solution)/shard_map/reduce_scatter | solution.py:109
  311.0 5.5 %all-to-all-start.1 = ((bf16[8,64,2048]{2,1,0:T(8,128)(2,1)}), bf16[8,64,2048]{2,1,0:T(8,128)(2,1)}, u32[]{:S(2)}, u32[]{:S(2)}) async-start(bf16[8,64,2048]{2,1,0:T(8,128)(2,1)} %bitcast.47), calls=%async_computation.3 | async-start | bytes 4194304 | tf_op jit(solution)/shard_map/all_to_all | solution.py:117
  316.6 0.1 reshape.212
  316.7 0.7 constant_dynamic-slice_fusion.2
  317.4 0.1 copy.19
  317.5 47.2 %all-to-all-done.1 = bf16[8,64,2048]{2,1,0:T(8,128)(2,1)} async-done(((bf16[8,64,2048]{2,1,0:T(8,128)(2,1)}), bf16[8,64,2048]{2,1,0:T(8,128)(2,1)}, u32[]{:S(2)}, u32[]{:S(2)}) %all-to-all-start.1) | async-done | bytes 2097184 | tf_op jit(solution)/shard_map/all_to_all | solution.py:117
  364.8 5.2 %gather_fusion.1 = bf16[256,2048]{1,0:T(8,128)(2,1)} fusion(bf16[512,2048]{1,0:T(8,128)(2,1)} %bitcast.20, s32[1024]{0:T(1024)S(1)} %pad_clamp_fusion), kind=kCustom, calls=%fused_computation.1 | custom fusion | bytes 2098176 | tf_op jit(solution)/shard_map/gather | solution.py:125
  370.0 3.4 reshape.229
  373.4 4.8 %multiply_reduce_fusion = f32[128,2048]{1,0:T(8,128)S(1)} fusion(f32[128,2,2048]{2,1,0:T(2,128)} %reshape.229, f32[128,2]{1,0:T(8,128)S(1)} %copy.19), kind=kLoop, calls=%fused_computation.10 | loop fusion | flops 786432 | bytes 3146752 | tf_op jit(solution)/shard_map/reduce_sum | solution.py:126
  378.3 1.0 add_convert_fusion
  (43 shorter events, 0.4 us)
Async XLA Ops:
  6.5 228.1 %copy-start = (bf16[1,512,2048]{2,1,0:T(8,128)(2,1)S(1)}, bf16[1,512,2048]{2,1,0:T(8,128)(2,1)}, u32[]{:S(2)}) copy-start(bf16[1,512,2048]{2,1,0:T(8,128)(2,1)} %param.23) | copy-start | bytes 6291460
  6.5 49.0 %reduce-scatter.3.cloned.1.call-start = ((), (), s32[]{:S(2)}) async-start(), calls=%async_computation.4 | async-start | bytes 2621440 | tf_op jit(solution)/shard_map/reduce_scatter | solution.py:83
  7.4 11.2 %collective-permute-start = (bf16[2,512]{1,0:T(2,128)(2,1)S(1)}, bf16[2,512]{1,0:T(2,128)(2,1)S(1)}, u32[]{:S(2)}, u32[]{:S(2)}) collective-permute-start(bf16[2,512]{1,0:T(2,128)(2,1)S(1)} %slice.28), channel_id=1, source_target_pairs={{0,4},{4,8},{8,12},{12,16},{16,20},{20,24},{24,28},{1,5},{5,9},{9,... | collective-permute-start | bytes 6152 | tf_op jit(solution)/shard_map/ppermute | solution.py:10
  13.0 5.6 %collective-permute-start.1 = (bf16[2,512]{1,0:T(2,128)(2,1)S(1)}, bf16[2,512]{1,0:T(2,128)(2,1)S(1)}, u32[]{:S(2)}, u32[]{:S(2)}) collective-permute-start(bf16[2,512]{1,0:T(2,128)(2,1)S(1)} %slice.29), channel_id=1, source_target_pairs={{0,4},{4,8},{8,12},{12,16},{16,20},{20,24},{24,28},{1,5},{5,9},{9,... | collective-permute-start | bytes 6152 | tf_op jit(solution)/shard_map/ppermute | solution.py:10
  18.6 37.0 %copy-start.6 = (bf16[128,2048]{1,0:T(8,128)(2,1)S(1)}, bf16[128,2048]{1,0:T(8,128)(2,1)}, u32[]{:S(2)}) copy-start(bf16[128,2048]{1,0:T(8,128)(2,1)} %param.17) | copy-start | bytes 1572868
  18.6 38.3 %copy-start.8 = (f32[2048]{0:T(1024)S(1)}, f32[2048]{0:T(1024)}, u32[]{:S(2)}) copy-start(f32[2048]{0:T(1024)} %param.18) | copy-start | bytes 24580
  23.2 287.8 %reduce-scatter.5.cloned.1.call-start = ((), (), s32[]{:S(2)}) async-start(), calls=%async_computation.5 | async-start | bytes 10485760 | tf_op jit(solution)/shard_map/reduce_scatter | solution.py:109
  115.2 1.3 copy-start.1
  116.5 25.5 %collective-permute-start.2 = (bf16[1,8,64,2048]{3,2,1,0:T(8,128)(2,1)S(1)}, bf16[1,8,64,2048]{3,2,1,0:T(8,128)(2,1)S(1)}, u32[]{:S(2)}, u32[]{:S(2)}) collective-permute-start(bf16[1,8,64,2048]{3,2,1,0:T(8,128)(2,1)S(1)} %bitcast.43), channel_id=1, source_target_pairs={{0,1},{1,2},{2,3},{3,0},{4,5},{5,6},{6,7},{7,4},{8,9},{9,10},{10,1... | collective-permute-start | bytes 6291464 | tf_op jit(solution)/shard_map/ppermute | solution.py:97
  141.9 1.3 copy-start.4
  143.3 25.6 %collective-permute-start.3 = (bf16[1,8,64,2048]{3,2,1,0:T(8,128)(2,1)S(1)}, bf16[1,8,64,2048]{3,2,1,0:T(8,128)(2,1)}, u32[]{:S(2)}, u32[]{:S(2)}) collective-permute-start(bf16[1,8,64,2048]{3,2,1,0:T(8,128)(2,1)S(1)} %collective-permute-done.2), channel_id=1, source_target_pairs={{0,1},{1,2},{2,3},{3,0},{4,5},{5,6},{6,7},{7,4},{8,9},{9,10},{10,1... | collective-permute-start | bytes 6291464 | tf_op jit(solution)/shard_map/ppermute | solution.py:97
  168.8 25.8 %collective-permute-start.4 = (bf16[1,8,64,2048]{3,2,1,0:T(8,128)(2,1)}, bf16[1,8,64,2048]{3,2,1,0:T(8,128)(2,1)}, u32[]{:S(2)}, u32[]{:S(2)}) collective-permute-start(bf16[1,8,64,2048]{3,2,1,0:T(8,128)(2,1)} %collective-permute-done.3), channel_id=1, source_target_pairs={{0,1},{1,2},{2,3},{3,0},{4,5},{5,6},{6,7},{7,4},{8,9},{9,10},{10,1... | collective-permute-start | bytes 6291464 | tf_op jit(solution)/shard_map/ppermute | solution.py:97
  168.8 32.3 %copy-start.5 = (bf16[1,8,64,2048]{3,2,1,0:T(8,128)(2,1)S(1)}, bf16[1,8,64,2048]{3,2,1,0:T(8,128)(2,1)}, u32[]{:S(2)}) copy-start(bf16[1,8,64,2048]{3,2,1,0:T(8,128)(2,1)} %copy-done.4) | copy-start | bytes 6291460
  197.8 4.8 %copy-start.2 = (bf16[1,8,64,2048]{3,2,0,1:T(8,128)(2,1)S(1)}, bf16[1,8,64,2048]{3,2,0,1:T(8,128)(2,1)}, u32[]{:S(2)}) copy-start(bf16[1,8,64,2048]{3,2,0,1:T(8,128)(2,1)} %copy-done.1) | copy-start | bytes 6291460
  213.4 8.4 %copy-start.9 = (bf16[1,2048,512]{2,1,0:T(8,128)(2,1)S(1)}, bf16[1,2048,512]{2,1,0:T(8,128)(2,1)}, u32[]{:S(2)}) copy-start(bf16[1,2048,512]{2,1,0:T(8,128)(2,1)} %param.21) | copy-start | bytes 6291460
  221.8 7.7 %copy-start.3 = (bf16[4,8,64,2048]{3,2,1,0:T(8,128)(2,1)S(1)}, bf16[4,8,64,2048]{3,2,1,0:T(8,128)(2,1)}, u32[]{:S(2)}) copy-start(bf16[4,8,64,2048]{3,2,1,0:T(8,128)(2,1)} %constant_dynamic-slice_fusion) | copy-start | bytes 25165828
  221.8 7.7 %copy-start.10 = (bf16[1,2048,512]{2,1,0:T(8,128)(2,1)S(1)}, bf16[1,2048,512]{2,1,0:T(8,128)(2,1)}, u32[]{:S(2)}) copy-start(bf16[1,2048,512]{2,1,0:T(8,128)(2,1)} %param.22) | copy-start | bytes 6291460
  311.0 53.7 %all-to-all-start.1 = ((bf16[8,64,2048]{2,1,0:T(8,128)(2,1)}), bf16[8,64,2048]{2,1,0:T(8,128)(2,1)}, u32[]{:S(2)}, u32[]{:S(2)}) async-start(bf16[8,64,2048]{2,1,0:T(8,128)(2,1)} %bitcast.47), calls=%async_computation.3 | async-start | bytes 4194304 | tf_op jit(solution)/shard_map/all_to_all | solution.py:117
  370.0 8.3 %copy-start.7 = (bf16[128,2048]{1,0:T(8,128)(2,1)S(1)}, bf16[128,2048]{1,0:T(8,128)(2,1)}, u32[]{:S(2)}) copy-start(bf16[128,2048]{1,0:T(8,128)(2,1)} %reduce-scatter.3.cloned.1.call-done) | copy-start | bytes 1572868
Sparse Core Ops, SparseCore 0:
  23.4 32.1 reduce-scatter.2
  241.5 69.4 reduce-scatter.4
